TPU v7x, 32 devices: a whole 2x2x4 slice. The times are simulated.
32 devices in a mesh: ep: 8 (over z, y), tp: 4 (over x, core).
Axes of the slice: x: 2, y: 2, z: 4, core: 2. Of those that a mesh axis runs over, the one named last changes fastest.
Arguments:
- tokens: bfloat16 [2048, 2048], P('ep'), may hold values from -6 to 6
- expert_ids: int32 [2048, 2], P('ep'), may hold values from 0 to 7, all different within a row; in each aligned block of 256 rows (0 to 255, 256 to 511, ...) at most 192 rows name the same one
- route_weight: float32 [2048, 2], P('ep'), may hold values from 0.1 to 1
- norm_gain: float32 [2048], replicated, may hold values from 0.1 to 1.9
- expert_gate: bfloat16 [8, 2048, 2048], P('ep', None, 'tp'), may hold values from -4 to 4
- expert_up: bfloat16 [8, 2048, 2048], P('ep', None, 'tp'), may hold values from -4 to 4
- expert_down: bfloat16 [8, 2048, 2048], P('ep', 'tp'), may hold values from -0.03125 to 0.03125
Outputs:
- combined: bfloat16 [2048, 2048], P('ep', 'tp')
Inputs may be any that keep to these rules, and one draw needn't show every extreme that they name: `expert_ids`: each row names 2 different experts. In each aligned block of 256 rows (the rows of one index of ep) no expert is named by more than 192 rows, and in some block one expert is named by exactly 192 rows.
All inputs are finite; a program needn't handle non-finite values.
Results may differ from a plain program's by a relative error of at most 0.012.
Values may be sent and summed in bfloat16 or wider, within the bound.
A program may use at most 128 MiB of HBM per device.

v0:
```python
import jax
import jax.numpy as jnp
from jax import lax
from jax.sharding import PartitionSpec as P

NORM_EPS = 1e-06
CLAMP_LIMIT = 7.0
SWISH_SCALE = 1.702


def normalize(tokens, norm_gain):
    values = tokens.astype(jnp.float32)
    scaled = values * lax.rsqrt(jnp.mean(values * values, axis=-1, keepdims=True) + NORM_EPS)
    return (scaled * norm_gain).astype(jnp.bfloat16)


def activate(gate_sum, up_sum):
    gate_cut = jnp.minimum(gate_sum, CLAMP_LIMIT)
    up_cut = jnp.clip(up_sum, -CLAMP_LIMIT, CLAMP_LIMIT)
    return ((up_cut + 1.0) * gate_cut * jax.nn.sigmoid(SWISH_SCALE * gate_cut)).astype(jnp.bfloat16)


def shards(tokens, expert_ids, route_weight, norm_gain, expert_gate, expert_up, expert_down):
    groups = lax.axis_size("ep")
    tp_count = lax.axis_size("tp")
    member_count = expert_gate.shape[0]
    experts = groups * member_count
    tok_count, model_width = tokens.shape
    top_count = expert_ids.shape[1]
    capacity = min(tok_count, 3 * tok_count * top_count // experts)
    quarter = model_width // tp_count
    normed = normalize(tokens, norm_gain)
    flat_ids = expert_ids.reshape(-1)
    onehot = (flat_ids[:, None] == jnp.arange(experts, dtype=jnp.int32)[None, :]).astype(jnp.int32)
    slot_index = jnp.sum(jnp.cumsum(onehot, axis=0) * onehot, axis=1) - 1
    position = flat_ids * capacity + slot_index
    token_index = jnp.arange(flat_ids.shape[0], dtype=jnp.int32) // top_count
    row_table = jnp.full((experts * capacity,), tok_count, jnp.int32).at[position].set(token_index)
    padded = jnp.concatenate([normed, jnp.zeros((1, model_width), jnp.bfloat16)], axis=0)
    offset = lax.axis_index("tp") * quarter
    source_rows = lax.dynamic_slice_in_dim(padded, offset, quarter, 1)
    send_rows = source_rows[row_table].reshape(groups, member_count, capacity, quarter)
    received = lax.all_to_all(send_rows, "ep", split_axis=0, concat_axis=0, tiled=True)
    slot_count = received.shape[2]
    shard_piece = lax.all_gather(received, "tp", axis=3, tiled=True)
    span_size = shard_piece.shape[3]
    member = 0
    row_block = shard_piece[:, member].reshape(-1, span_size)
    gate_rows = expert_gate[member]
    up_rows = expert_up[member]
    gate_list = [jnp.dot(row_block, gate_rows, preferred_element_type=jnp.float32)]
    up_list = [jnp.dot(row_block, up_rows, preferred_element_type=jnp.float32)]
    gate_sum = jnp.stack(gate_list)
    up_sum = jnp.stack(up_list)
    activated = activate(gate_sum, up_sum)
    member = 0
    weight_rows = expert_down[member]
    product = lax.dot_general(
        weight_rows, activated[member], (((0,), (1,)), ((), ())), preferred_element_type=jnp.float32
    )
    term_list = [product.reshape(quarter * lax.axis_size("tp"), groups, slot_count)]
    summed = lax.psum_scatter(
        jnp.stack(term_list, axis=2).astype(jnp.bfloat16), "tp", scatter_dimension=0, tiled=True
    )
    returned = lax.all_to_all(
        summed.reshape(quarter, experts * capacity), "ep", split_axis=1, concat_axis=1, tiled=True
    )
    picked = jnp.take(returned, position, axis=1).reshape(quarter, tok_count, top_count)
    weighted = jnp.sum(picked.astype(jnp.float32) * route_weight[None, :, :], axis=2)
    return weighted.T.astype(jnp.bfloat16)


def solution(mesh):
    return jax.shard_map(
        shards,
        mesh=mesh,
        in_specs=(
            P("ep", None),
            P("ep", None),
            P("ep", None),
            P(),
            P("ep", None, "tp"),
            P("ep", None, "tp"),
            P("ep", "tp", None),
        ),
        out_specs=P("ep", "tp"),
        check_vma=False,
    )
```

profile of v0, /device:TPU:0, one launch (start us, length us, event | category | flops | bytes accessed | tf_op | source)
XLA Modules:
  0.0 245.8 jit_solution(14064720156240668413)
XLA Ops:
  6.5 0.0 copy-start
  6.5 0.0 all-gather.2.cloned.1.call-start
  6.5 1.0 copy.19
  7.5 0.1 eq.26
  7.7 0.1 reshape.111
  7.8 0.7 broadcast_multiply_fusion
  8.5 1.1 reduce-window.6
  9.6 0.2 slice_reduce_fusion
  9.9 0.1 fusion.12
  10.0 0.1 copy.23
  10.1 0.1 mul.76
  10.3 2.5 scatter_custom_fusion
  12.8 1.5 fusion.4
  14.3 1.5 fusion.6
  15.9 5.4 %gather_fusion = bf16[1536,512]{1,0:T(8,128)(2,1)} fusion(bf16[257,512]{1,0:T(8,128)(2,1)S(1)} %pad_dynamic-slice_fusion, s32[2048]{0:T(1024)S(1)} %pad_clamp_fusion), kind=kCustom, calls=%fused_computation | custom fusion | bytes 3151872 | tf_op jit(solution)/shard_map/gather | solution.py:42
  21.3 44.4 %all_to_all.17 = bf16[8,1,192,512]{3,2,1,0:T(8,128)(2,1)} all-to-all(bf16[8,1,192,512]{3,2,1,0:T(8,128)(2,1)} %bitcast.37), channel_id=1, replica_groups=mesh['ep'=8,'tp'=4] {'ep'}, dimensions={0} | all-to-all | bytes 3145728 | tf_op jit(solution)/shard_map/all_to_all | solution.py:43
  65.7 0.0 all-gather.2.cloned.1.call-update
  65.8 0.0 reduce-scatter.2.cloned.1.call-start
  65.8 45.5 %all-gather.2.cloned.1.call-done = bf16[8,1,192,2048]{3,2,1,0:T(8,128)(2,1)} async-done(((bf16[8,1,192,512]{3,2,1,0:T(8,128)(2,1)}), bf16[8,1,192,2048]{3,2,1,0:T(8,128)(2,1)}) %all-gather.2.cloned.1.call-update) | async-done | bytes 6291472 | tf_op jit(solution)/shard_map/all_gather | solution.py:45
  111.3 8.5 %convolution_minimum_fusion = f32[1536,512]{1,0:T(8,128)} fusion(bf16[1536,2048]{1,0:T(8,128)(2,1)} %bitcast.43, bf16[1,2048,512]{2,1,0:T(8,128)(2,1)} %param.11), kind=kOutput, calls=%fused_computation.5 | convolution fusion | flops 3222011904 | bytes 11534336 | tf_op jit(solution)/shard_map/dot_general | solution.py:51
  119.8 0.0 copy-done
  119.8 11.9 %convolution_convert_fusion = bf16[1536,2048]{1,0:T(8,128)(2,1)} fusion(bf16[1,512,2048]{2,1,0:T(8,128)(2,1)S(1)} %copy-done, f32[1536,512]{1,0:T(8,128)} %convolution_minimum_fusion, bf16[1536,2048]{1,0:T(8,128)(2,1)} %bitcast.44, bf16[1,2048,512]{2,1,0:T(8,128)(2,1)} %param.12), kind=kOutput, calls=%fused_computation.3 | convolution fusion | flops 6452674560 | bytes 19922944 | tf_op jit(solution)/shard_map/dot_general | solution.py:58
  131.7 0.0 reduce-scatter.2.cloned.1.call-update
  131.7 0.0 copy-start.1
  131.7 0.0 copy-start.2
  131.7 58.0 %reduce-scatter.2.cloned.1.call-done = bf16[512,8,1,192]{0,3,1,2:T(8,128)(2,1)} async-done(((bf16[2048,8,1,192]{0,3,1,2:T(8,128)(2,1)}), bf16[512,8,1,192]{0,3,1,2:T(8,128)(2,1)}) %reduce-scatter.2.cloned.1.call-update) | async-done | bytes 1572880 | tf_op jit(solution)/shard_map/reduce_scatter | solution.py:62
  189.7 5.5 %all-to-all-start.1 = ((bf16[512,8,192]{0,2,1:T(8,128)(2,1)}), bf16[512,8,192]{0,2,1:T(8,128)(2,1)}, u32[]{:S(2)}, u32[]{:S(2)}) async-start(bf16[512,8,192]{0,2,1:T(8,128)(2,1)} %bitcast.39), calls=%async_computation.2 | async-start | bytes 3145728 | tf_op jit(solution)/shard_map/all_to_all | solution.py:65
  195.2 0.1 sub.15
  195.4 0.1 copy.21
  195.5 0.0 copy-done.1
  195.5 0.2 copy.22
  195.7 0.0 copy-done.2
  195.7 0.1 copy.25
  195.8 36.3 %all-to-all-done.1 = bf16[512,8,192]{0,2,1:T(8,128)(2,1)} async-done(((bf16[512,8,192]{0,2,1:T(8,128)(2,1)}), bf16[512,8,192]{0,2,1:T(8,128)(2,1)}, u32[]{:S(2)}, u32[]{:S(2)}) %all-to-all-start.1) | async-done | bytes 1572896 | tf_op jit(solution)/shard_map/all_to_all | solution.py:65
  232.2 3.6 %gather_fusion.1 = bf16[512,512]{1,0:T(8,128)(2,1)S(1)} fusion(bf16[512,1536]{0,1:T(8,128)(2,1)} %bitcast.13, s32[1024]{0:T(1024)S(1)} %pad_clamp_fusion.1), kind=kCustom, calls=%fused_computation.1 | custom fusion | bytes 1050624 | tf_op jit(solution)/shard_map/jit(_take)/gather | solution.py:68
  235.8 0.2 gather.11
  236.0 2.9 %multiply_reduce_fusion = bf16[512,256]{0,1:T(8,128)(2,1)} fusion(bf16[512,256,2]{0,2,1:T(2,128)(2,1)S(1)} %gather.11, pred[256,2]{1,0:T(8,128)(4,1)S(1)} %copy.22, f32[256,2]{1,0:T(8,128)S(1)} %copy.25), kind=kLoop, calls=%fused_computation.19 | loop fusion | flops 917504 | bytes 788992 | tf_op jit(solution)/shard_map/reduce_sum | solution.py:69
  (12 shorter events, 0.1 us)
Async XLA Ops:
  6.5 113.3 %copy-start = (bf16[1,512,2048]{2,1,0:T(8,128)(2,1)S(1)}, bf16[1,512,2048]{2,1,0:T(8,128)(2,1)}, u32[]{:S(2)}) copy-start(bf16[1,512,2048]{2,1,0:T(8,128)(2,1)} %param.13) | copy-start | bytes 6291460
  6.5 104.7 %all-gather.2.cloned.1.call-start = ((), (), s32[]{:S(2)}) async-start(), calls=%async_computation.3 | async-start | bytes 7864320 | tf_op jit(solution)/shard_map/all_gather | solution.py:45
  65.8 124.0 %reduce-scatter.2.cloned.1.call-start = ((), (), s32[]{:S(2)}) async-start(), calls=%async_computation.4 | async-start | bytes 7864320 | tf_op jit(solution)/shard_map/reduce_scatter | solution.py:62
  131.7 63.8 %copy-start.1 = (s32[256,2]{0,1:T(2,128)S(1)}, s32[256,2]{0,1:T(2,128)}, u32[]{:S(2)}) copy-start(s32[256,2]{0,1:T(2,128)} %param.8) | copy-start | bytes 6148
  131.7 64.0 %copy-start.2 = (f32[256,2]{0,1:T(2,128)S(1)}, f32[256,2]{0,1:T(2,128)}, u32[]{:S(2)}) copy-start(f32[256,2]{0,1:T(2,128)} %param.9) | copy-start | bytes 6148
  189.7 42.4 %all-to-all-start.1 = ((bf16[512,8,192]{0,2,1:T(8,128)(2,1)}), bf16[512,8,192]{0,2,1:T(8,128)(2,1)}, u32[]{:S(2)}, u32[]{:S(2)}) async-start(bf16[512,8,192]{0,2,1:T(8,128)(2,1)} %bitcast.39), calls=%async_computation.2 | async-start | bytes 3145728 | tf_op jit(solution)/shard_map/all_to_all | solution.py:65
Sparse Core Ops, SparseCore 0:
  65.9 45.3 all-gather.1
  131.8 57.8 reduce-scatter.1
where the time goes:
time: 246 us
  waiting for transfers between devices  140 us (57%)
  blocking collectives  44.4 us (18%)
  matrix products  20.4 us (8%)
  local copies, waits for them, and re-layouts  14 us (6%)
  between operations  13.6 us (6%)
  other arithmetic  8.01 us (3%)
  starting transfers between devices  5.56 us (2%)
    reduce_scatter x1, waiting for transfers between devices, shards(): lax.psum_scatter(jnp.stack(term_list, axis=2).astype(jnp.bfloat16), 'tp',...  58 us
    all_gather x1, waiting for transfers between devices, shards(): shard_piece = lax.all_gather(received, 'tp', axis=3, tiled=True)  45.5 us
    all_to_all x1, blocking collectives, shards(): lax.all_to_all(send_rows, 'ep', split_axis=0, concat_axis=0, tiled=True)  44.4 us
    all_to_all x1, waiting for transfers between devices, shards(): lax.all_to_all(summed.reshape(quarter, experts * capacity), 'ep', split_a...  36.3 us
    dot_general x1, matrix products, shards(): lax.dot_general(weight_rows, activated[member], (((0,), (1,)), ((), ())),...  11.9 us
    dot_general x1, matrix products, shards(): jnp.dot(row_block, gate_rows, preferred_element_type=jnp.float32)  8.52 us
    all_to_all x1, starting transfers between devices, shards(): lax.all_to_all(summed.reshape(quarter, experts * capacity), 'ep', split_a...  5.51 us
    gather x1, local copies, waits for them, and re-layouts, shards(): source_rows[row_table].reshape(groups, member_count, capacity, quarter)  5.43 us
  transfers between devices with their start and end apart: 3, of which 3 were waited for; matrix products, arithmetic and copies ran while one was open for 0% of the time, Pallas kernels for 0%

commit v1 on v0

--- a/solution.py
+++ b/solution.py
@@ -62,9 +62,10 @@
     summed = lax.psum_scatter(
         jnp.stack(term_list, axis=2).astype(jnp.bfloat16), "tp", scatter_dimension=0, tiled=True
     )
-    returned = lax.all_to_all(
-        summed.reshape(quarter, experts * capacity), "ep", split_axis=1, concat_axis=1, tiled=True
-    )
+    block = summed.reshape(quarter, experts * capacity)
+    pieces = jnp.split(block, lax.axis_size("ep"), axis=1)
+    incoming = lax.all_to_all(jnp.stack(pieces), "ep", 0, 0)
+    returned = jnp.concatenate(incoming, axis=1)
     picked = jnp.take(returned, position, axis=1).reshape(quarter, tok_count, top_count)
     weighted = jnp.sum(picked.astype(jnp.float32) * route_weight[None, :, :], axis=2)
     return weighted.T.astype(jnp.bfloat16)

time: 246 us -> 259 us (1.053)
  local copies, waits for them, and re-layouts: 14 us -> 26.9 us
    unnamed x8 -> x17, local copies, waits for them, and re-layouts: 1.11 us -> 12.4 us
where the time goes in v1:
time: 259 us; the launch traced here: 258 us
  waiting for transfers between devices  140 us (54%)
  blocking collectives  44.4 us (17%)
  local copies, waits for them, and re-layouts  26.9 us (10%)
  matrix products  20.4 us (8%)
  between operations  13.6 us (5%)
  other arithmetic  7.47 us (3%)
  starting transfers between devices  5.56 us (2%)
    reduce_scatter x1, waiting for transfers between devices, shards(): lax.psum_scatter(jnp.stack(term_list, axis=2).astype(jnp.bfloat16), 'tp',...  58 us
    all_gather x1, waiting for transfers between devices, shards(): shard_piece = lax.all_gather(received, 'tp', axis=3, tiled=True)  45.5 us
    all_to_all x1, blocking collectives, shards(): lax.all_to_all(send_rows, 'ep', split_axis=0, concat_axis=0, tiled=True)  44.4 us
    all_to_all x1, waiting for transfers between devices, shards(): incoming = lax.all_to_all(jnp.stack(pieces), 'ep', 0, 0)  36.4 us
    unnamed x17, local copies, waits for them, and re-layouts  12.4 us
    dot_general x1, matrix products, shards(): lax.dot_general(weight_rows, activated[member], (((0,), (1,)), ((), ())),...  11.9 us
    dot_general x1, matrix products, shards(): jnp.dot(row_block, gate_rows, preferred_element_type=jnp.float32)  8.52 us
    all_to_all x1, starting transfers between devices, shards(): incoming = lax.all_to_all(jnp.stack(pieces), 'ep', 0, 0)  5.52 us
  transfers between devices with their start and end apart: 3, of which 3 were waited for; matrix products, arithmetic and copies ran while one was open for 0% of the time, Pallas kernels for 0%

profile of v1, /device:TPU:0, one launch (start us, length us, event | category | flops | bytes accessed | tf_op | source)
XLA Modules:
  0.0 258.2 jit_solution(4329248123373415777)
XLA Ops:
  6.5 0.0 copy-start
  6.5 0.0 copy-start.1
  6.5 0.0 all-gather.2.cloned.1.call-start
  6.5 1.0 copy.19
  7.5 0.1 eq.26
  7.7 0.1 reshape.116
  7.8 0.7 broadcast_multiply_fusion
  8.5 1.1 reduce-window.6
  9.6 0.2 slice_reduce_fusion
  9.9 0.1 fusion.20
  10.0 0.1 copy.23
  10.1 0.1 mul.76
  10.3 2.5 scatter_custom_fusion
  12.8 1.5 fusion.4
  14.3 0.0 copy-done.1
  14.3 1.0 fusion.6
  15.4 5.4 %gather_fusion = bf16[1536,512]{1,0:T(8,128)(2,1)} fusion(bf16[257,512]{1,0:T(8,128)(2,1)S(1)} %pad_dynamic-slice_fusion, s32[2048]{0:T(1024)S(1)} %pad_clamp_fusion), kind=kCustom, calls=%fused_computation | custom fusion | bytes 3151872 | tf_op jit(solution)/shard_map/gather | solution.py:42
  20.8 44.4 %all_to_all.10 = bf16[8,1,192,512]{3,2,1,0:T(8,128)(2,1)} all-to-all(bf16[8,1,192,512]{3,2,1,0:T(8,128)(2,1)} %bitcast.71), channel_id=1, replica_groups=mesh['ep'=8,'tp'=4] {'ep'}, dimensions={0} | all-to-all | bytes 3145728 | tf_op jit(solution)/shard_map/all_to_all | solution.py:43
  65.2 0.0 all-gather.2.cloned.1.call-update
  65.2 0.0 reduce-scatter.2.cloned.1.call-start
  65.3 45.5 %all-gather.2.cloned.1.call-done = bf16[8,1,192,2048]{3,2,1,0:T(8,128)(2,1)} async-done(((bf16[8,1,192,512]{3,2,1,0:T(8,128)(2,1)}), bf16[8,1,192,2048]{3,2,1,0:T(8,128)(2,1)}) %all-gather.2.cloned.1.call-update) | async-done | bytes 6291472 | tf_op jit(solution)/shard_map/all_gather | solution.py:45
  110.8 8.5 %convolution_minimum_fusion = f32[1536,512]{1,0:T(8,128)} fusion(bf16[1536,2048]{1,0:T(8,128)(2,1)} %bitcast.84, bf16[1,2048,512]{2,1,0:T(8,128)(2,1)} %param.11), kind=kOutput, calls=%fused_computation.5 | convolution fusion | flops 3222011904 | bytes 11534336 | tf_op jit(solution)/shard_map/dot_general | solution.py:51
  119.3 0.0 copy-done
  119.3 11.9 %convolution_convert_fusion = bf16[1536,2048]{1,0:T(8,128)(2,1)} fusion(bf16[1,512,2048]{2,1,0:T(8,128)(2,1)S(1)} %copy-done, f32[1536,512]{1,0:T(8,128)} %convolution_minimum_fusion, bf16[1536,2048]{1,0:T(8,128)(2,1)} %bitcast.85, bf16[1,2048,512]{2,1,0:T(8,128)(2,1)} %param.12), kind=kOutput, calls=%fused_computation.3 | convolution fusion | flops 6452674560 | bytes 19922944 | tf_op jit(solution)/shard_map/dot_general | solution.py:58
  131.2 0.0 reduce-scatter.2.cloned.1.call-update
  131.2 58.0 %reduce-scatter.2.cloned.1.call-done = bf16[512,8,1,192]{0,3,1,2:T(8,128)(2,1)} async-done(((bf16[2048,8,1,192]{0,3,1,2:T(8,128)(2,1)}), bf16[512,8,1,192]{0,3,1,2:T(8,128)(2,1)}) %reduce-scatter.2.cloned.1.call-update) | async-done | bytes 1572880 | tf_op jit(solution)/shard_map/reduce_scatter | solution.py:62
  189.2 1.6 fusion.19
  190.8 1.6 fusion.18
  192.4 1.6 fusion.17
  194.0 1.6 fusion.16
  195.6 1.6 fusion.15
  197.2 1.6 fusion.14
  198.9 0.0 copy-start.2
  198.9 0.0 copy-start.3
  198.9 1.6 fusion.13
  200.5 1.6 fusion.12
  202.1 5.5 %all-to-all-start.1 = ((bf16[8,512,192]{1,2,0:T(8,128)(2,1)}), bf16[8,512,192]{1,2,0:T(8,128)(2,1)}, u32[]{:S(2)}, u32[]{:S(2)}) async-start(bf16[8,512,192]{1,2,0:T(8,128)(2,1)} %fusion.12), calls=%async_computation.2 | async-start | bytes 3145728 | tf_op jit(solution)/shard_map/all_to_all | solution.py:67
  207.6 0.1 sub.15
  207.8 0.1 copy.21
  207.9 0.0 copy-done.2
  207.9 0.2 copy.22
  208.1 0.0 copy-done.3
  208.1 0.1 copy.25
  208.2 36.4 %all-to-all-done.1 = bf16[8,512,192]{1,2,0:T(8,128)(2,1)} async-done(((bf16[8,512,192]{1,2,0:T(8,128)(2,1)}), bf16[8,512,192]{1,2,0:T(8,128)(2,1)}, u32[]{:S(2)}, u32[]{:S(2)}) %all-to-all-start.1) | async-done | bytes 1572896 | tf_op jit(solution)/shard_map/all_to_all | solution.py:67
  244.6 3.6 %gather_fusion.1 = bf16[512,512]{1,0:T(8,128)(2,1)S(1)} fusion(bf16[512,1536]{0,1:T(8,128)(2,1)} %bitcast.22, s32[1024]{0:T(1024)S(1)} %pad_clamp_fusion.1), kind=kCustom, calls=%fused_computation.1 | custom fusion | bytes 1050624 | tf_op jit(solution)/shard_map/jit(_take)/gather | solution.py:69
  248.2 0.2 gather.11
  248.4 2.9 %multiply_reduce_fusion = bf16[512,256]{0,1:T(8,128)(2,1)} fusion(bf16[512,256,2]{0,2,1:T(2,128)(2,1)S(1)} %gather.11, pred[256,2]{1,0:T(8,128)(4,1)S(1)} %copy.22, f32[256,2]{1,0:T(8,128)S(1)} %copy.25), kind=kLoop, calls=%fused_computation.19 | loop fusion | flops 917504 | bytes 788992 | tf_op jit(solution)/shard_map/reduce_sum | solution.py:70
  (12 shorter events, 0.1 us)
Async XLA Ops:
  6.5 112.7 %copy-start = (bf16[1,512,2048]{2,1,0:T(8,128)(2,1)S(1)}, bf16[1,512,2048]{2,1,0:T(8,128)(2,1)}, u32[]{:S(2)}) copy-start(bf16[1,512,2048]{2,1,0:T(8,128)(2,1)} %param.13) | copy-start | bytes 6291460
  6.5 7.8 %copy-start.1 = (bf16[256,2048]{1,0:T(8,128)(2,1)S(1)}, bf16[256,2048]{1,0:T(8,128)(2,1)}, u32[]{:S(2)}) copy-start(bf16[256,2048]{1,0:T(8,128)(2,1)} %param.7) | copy-start | bytes 3145732
  6.5 104.2 %all-gather.2.cloned.1.call-start = ((), (), s32[]{:S(2)}) async-start(), calls=%async_computation.3 | async-start | bytes 7864320 | tf_op jit(solution)/shard_map/all_gather | solution.py:45
  65.2 124.0 %reduce-scatter.2.cloned.1.call-start = ((), (), s32[]{:S(2)}) async-start(), calls=%async_computation.4 | async-start | bytes 7864320 | tf_op jit(solution)/shard_map/reduce_scatter | solution.py:62
  198.9 9.0 %copy-start.2 = (s32[256,2]{0,1:T(2,128)S(1)}, s32[256,2]{0,1:T(2,128)}, u32[]{:S(2)}) copy-start(s32[256,2]{0,1:T(2,128)} %param.8) | copy-start | bytes 6148
  198.9 9.2 %copy-start.3 = (f32[256,2]{0,1:T(2,128)S(1)}, f32[256,2]{0,1:T(2,128)}, u32[]{:S(2)}) copy-start(f32[256,2]{0,1:T(2,128)} %param.9) | copy-start | bytes 6148
  202.1 42.5 %all-to-all-start.1 = ((bf16[8,512,192]{1,2,0:T(8,128)(2,1)}), bf16[8,512,192]{1,2,0:T(8,128)(2,1)}, u32[]{:S(2)}, u32[]{:S(2)}) async-start(bf16[8,512,192]{1,2,0:T(8,128)(2,1)} %fusion.12), calls=%async_computation.2 | async-start | bytes 3145728 | tf_op jit(solution)/shard_map/all_to_all | solution.py:67
Sparse Core Ops, SparseCore 0:
  65.4 45.3 all-gather.1
  131.3 57.8 reduce-scatter.1
